TPU v7x, 32 devices: a whole 2x2x4 slice. The times are simulated.
32 devices in a mesh: grp: 2 (over y), ep: 4 (over z), tp: 4 (over x, core).
Axes of the slice: x: 2, y: 2, z: 4, core: 2. Of those that a mesh axis runs over, the one named last changes fastest.
Arguments:
- queries: bfloat16 [2048, 2048], P(('grp', 'ep'), 'tp'), parts along dimension 0, may hold values from -8 to 8
- keys: bfloat16 [2048, 512], P(('grp', 'ep')), parts along dimension 0, may hold values from -8 to 8
- values: bfloat16 [2048, 512], P(('grp', 'ep')), parts along dimension 0, may hold values from -6 to 6
- q_gain: float32 [128], replicated, may hold values from 0.6 to 5.8
- k_gain: float32 [128], replicated, may hold values from 0.6 to 5.8
- w_out: bfloat16 [2048, 2048], P(None, 'tp'), may hold values from -0.125 to 0.125
- moe_rows: bfloat16 [1536, 2048], P(('grp', 'ep')), parts along dimension 0, may hold values from -6 to 6
- routes: int32 [1536, 2], P(('grp', 'ep')), parts along dimension 0, may hold values from 0 to 3, all different within a row; in each aligned block of 192 rows (0 to 191, 192 to 383, ...) at most 144 rows name the same one
- group_gate: float32 [1536], P(('grp', 'ep')), parts along dimension 0, may hold values from 0.25 to 1
- expert_logits: float32 [1536, 2], P(('grp', 'ep')), parts along dimension 0, may hold values from -6 to 6
- moe_gain: float32 [2048], replicated, may hold values from 0.1 to 1.9
- w_gate: bfloat16 [4, 2048, 2048], P('ep', None, 'tp'), may hold values from -0.125 to 0.125
- w_up: bfloat16 [4, 2048, 2048], P('ep', None, 'tp'), may hold values from -0.125 to 0.125
- w_down: bfloat16 [4, 2048, 2048], P('ep', 'tp'), may hold values from -0.125 to 0.125
Outputs:
- attn_out: bfloat16 [2048, 2048], P(('grp', 'ep'), 'tp'), parts along dimension 0
- moe_out: bfloat16 [1536, 2048], P(('grp', 'ep'), 'tp'), parts along dimension 0
There are 2 independent parts, one for each index of `grp`. A program takes and returns all parts, laid end to end along the dimension named above; an argument that names none is the same for every part. Nothing has to cross between parts.
Inputs may be any that keep to these rules, and one draw needn't show every extreme that they name: `routes`: each row names 2 different experts; within the rows of one index of ep no expert is named more than 144 times, a bound that some block reaches.
All inputs are finite; a program needn't handle non-finite values.
Results may differ from a plain program's by a relative error of at most 0.019.
The roundings to bfloat16 on the way count: a program that leaves them out, or rounds other values in their place, can miss the bound.
Values may be sent and summed in bfloat16 or wider, within the bound.
A program may use at most 64 MiB of HBM per device.

v0:
```python
import jax
import jax.numpy as jnp
from jax import lax
from jax.sharding import PartitionSpec as P

HEADS = 16
KV_HEADS = 4
HEAD_DIM = 128
GRID_W = 64
TOPK = 2


def head_norm(x, gain):
    wide = x.astype(jnp.float32)
    return wide * lax.rsqrt(jnp.mean(wide * wide, axis=-1, keepdims=True) + 1e-06) * gain


def rotate(x, first):
    count = x.shape[0]
    pos = first + jnp.arange(count, dtype=jnp.int32)
    row = (pos // GRID_W).astype(jnp.float32)
    col = (pos % GRID_W).astype(jnp.float32)
    nfreq = HEAD_DIM // 4
    inverse = 10000.0 ** (-jnp.arange(nfreq, dtype=jnp.float32) / nfreq)
    angle = jnp.concatenate(
        [
            row[:, None] * inverse,
            row[:, None] * inverse,
            col[:, None] * inverse,
            col[:, None] * inverse,
        ],
        axis=1,
    )
    parts = x.reshape(x.shape[:-1] + (2, 2, nfreq))
    turned = jnp.stack([-parts[..., 1, :], parts[..., 0, :]], axis=-2).reshape(x.shape)
    return x * jnp.cos(angle)[:, None, :] + turned * jnp.sin(angle)[:, None, :]


def per_device(
    queries,
    keys,
    values,
    q_gain,
    k_gain,
    w_out,
    moe_rows,
    routes,
    group_gate,
    expert_logits,
    moe_gain,
    w_gate,
    w_up,
    w_down,
):
    rows = queries.shape[0]
    heads_dev = queries.shape[1] // HEAD_DIM
    group = HEADS // KV_HEADS
    kv_dev = max(1, heads_dev // group)
    per_kv = heads_dev // kv_dev
    first_kv = lax.axis_index("tp") * heads_dev // group
    first_row = lax.axis_index("ep") * rows
    k_mine = lax.dynamic_slice_in_dim(keys, first_kv * HEAD_DIM, kv_dev * HEAD_DIM, 1)
    v_mine = lax.dynamic_slice_in_dim(values, first_kv * HEAD_DIM, kv_dev * HEAD_DIM, 1)
    k_rot = rotate(head_norm(k_mine.reshape(rows, kv_dev, HEAD_DIM), k_gain), first_row)
    k_rot = k_rot.astype(jnp.bfloat16).reshape(rows, kv_dev * HEAD_DIM)
    q_rot = rotate(head_norm(queries.reshape(rows, heads_dev, HEAD_DIM), q_gain), first_row)
    q_rot = q_rot.astype(jnp.bfloat16).reshape(rows, kv_dev, per_kv, HEAD_DIM)
    scale = HEAD_DIM ** (-0.5)
    top = jnp.full((rows, kv_dev, per_kv), -jnp.inf, jnp.float32)
    total = jnp.zeros((rows, kv_dev, per_kv), jnp.float32)
    acc = jnp.zeros((rows, kv_dev, per_kv, HEAD_DIM), jnp.float32)
    k_piece = lax.all_gather(k_rot, "ep", axis=0, tiled=True)
    v_piece = lax.all_gather(v_mine, "ep", axis=0, tiled=True)
    count = k_piece.shape[0]
    key_rows = k_piece.reshape(count, kv_dev, HEAD_DIM)
    value_rows = v_piece.reshape(count, kv_dev, HEAD_DIM)
    scores = (
        jnp.einsum("qkgd,nkd->qkgn", q_rot, key_rows, preferred_element_type=jnp.float32) * scale
    )
    new_top = jnp.max(scores, axis=-1)
    shrink = jnp.exp(top - new_top)
    expo = jnp.exp(scores - new_top[..., None])
    total = total * shrink + jnp.sum(expo, axis=-1)
    acc = acc * shrink[..., None] + jnp.einsum(
        "qkgn,nkd->qkgd", expo.astype(jnp.bfloat16), value_rows, preferred_element_type=jnp.float32
    )
    top, total, acc = (new_top, total, acc)
    mixed = (acc / total[..., None]).astype(jnp.bfloat16).reshape(rows, heads_dev * HEAD_DIM)
    attn_out = jnp.dot(
        lax.all_gather(mixed, "tp", axis=1, tiled=True), w_out, preferred_element_type=jnp.float32
    ).astype(jnp.bfloat16)
    count = moe_rows.shape[0]
    width = moe_rows.shape[1]
    peers = lax.axis_size("ep")
    capacity = 3 * count // peers
    wide = moe_rows.astype(jnp.float32)
    normed = (
        wide * lax.rsqrt(jnp.mean(wide * wide, axis=-1, keepdims=True) + 1e-06) * moe_gain
    ).astype(jnp.bfloat16)
    chosen = routes.reshape(-1)
    onehot = (chosen[:, None] == jnp.arange(peers, dtype=jnp.int32)[None, :]).astype(jnp.int32)
    rank = jnp.sum((jnp.cumsum(onehot, axis=0) - onehot) * onehot, axis=1)
    slots = chosen * capacity + rank
    owner = jnp.arange(count * TOPK, dtype=jnp.int32) // TOPK
    source = jnp.zeros((peers * capacity,), jnp.int32).at[slots].set(owner)
    used = jnp.zeros((peers * capacity,), jnp.bool_).at[slots].set(True)
    outgoing = jnp.where(used[:, None], normed[source], jnp.zeros((), jnp.bfloat16)).reshape(
        peers, capacity, width
    )
    part_cols = width // lax.axis_size("tp")
    mine = lax.dynamic_slice_in_dim(outgoing, lax.axis_index("tp") * part_cols, part_cols, 2)
    arrived = lax.all_gather(
        lax.all_to_all(mine, "ep", split_axis=0, concat_axis=0, tiled=True),
        "tp",
        axis=2,
        tiled=True,
    )
    first_dim, second_dim, cols = arrived.shape
    flat = arrived.reshape(first_dim * second_dim, cols)
    gate = jnp.dot(flat, w_gate[0], preferred_element_type=jnp.float32)
    up = jnp.dot(flat, w_up[0], preferred_element_type=jnp.float32)
    hidden = (jax.nn.silu(gate) * up).astype(jnp.bfloat16)
    result = jnp.dot(hidden, w_down[0], preferred_element_type=jnp.float32).astype(jnp.bfloat16)
    partial_value = result.reshape(first_dim, second_dim, cols)
    summed = (
        lax.psum_scatter(partial_value, "tp", scatter_dimension=2, tiled=True)
        .astype(jnp.float32)
        .astype(jnp.bfloat16)
    )
    back = lax.all_to_all(summed, "ep", split_axis=0, concat_axis=0, tiled=True)
    back = back.reshape(peers * capacity, back.shape[2])
    picked = back[slots].astype(jnp.float32).reshape(count, TOPK, back.shape[1])
    weights = group_gate[:, None] * jax.nn.softmax(expert_logits, axis=-1)
    moe_out = jnp.sum(weights[:, :, None] * picked, axis=1).astype(jnp.bfloat16)
    return (attn_out, moe_out)


def solution(mesh):
    placed = (
        P(("grp", "ep"), "tp"),
        P(("grp", "ep"), None),
        P(("grp", "ep"), None),
        P(),
        P(),
        P(None, "tp"),
        P(("grp", "ep"), None),
        P(("grp", "ep"), None),
        P(("grp", "ep")),
        P(("grp", "ep"), None),
        P(),
        P("ep", None, "tp"),
        P("ep", None, "tp"),
        P("ep", "tp", None),
    )
    return jax.shard_map(
        per_device,
        mesh=mesh,
        in_specs=placed,
        out_specs=(P(("grp", "ep"), "tp"), P(("grp", "ep"), "tp")),
        check_vma=False,
    )
```

profile of v0, /device:TPU:0, one launch (start us, length us, event | category | flops | bytes accessed | tf_op | source)
XLA Modules:
  0.0 148.1 jit_solution(11262557061539180350)
XLA Ops:
  7.2 0.0 copy-start
  7.2 0.0 all-gather.5.cloned.1.call-start
  7.2 0.9 copy.30
  8.2 0.1 eq.32
  8.3 0.1 eq.28
  8.5 0.7 broadcast_multiply_fusion.2
  9.2 1.2 reduce-window.6
  10.4 0.2 slice_reduce_fusion
  10.6 0.2 reduce-window.9
  10.8 0.1 add_bitcast_fusion
  10.8 0.1 copy.29
  11.0 0.1 mul.316
  11.2 2.9 %scatter_custom_fusion.1 = s32[576]{0:T(1024)S(1)} fusion(s32[384]{0:T(512)S(1)} %fusion.58, s32[384]{0:T(512)S(1)} %add_select_fusion, s32[]{:T(128)} %constant.95.clone.1), kind=kCustom, calls=%fused_computation.81 | custom fusion | bytes 2308 | tf_op jit(solution)/shard_map/scatter | solution.py:105
  14.1 1.4 fusion.13
  15.5 2.0 %scatter_custom_fusion = pred[576]{0:T(1024)(128)(4,1)S(1)} fusion(s32[384]{0:T(512)S(1)} %fusion.58, pred[384]{0:T(512)(128)(4,1)S(1)} %broadcast.278, pred[]{:T(512)} %constant.115.clone.1), kind=kCustom, calls=%fused_computation.86 | custom fusion | bytes 577 | tf_op jit(solution)/shard_map/scatter | solution.py:106
  17.5 0.1 broadcast_in_dim.24
  17.6 1.4 fusion.15
  19.0 4.0 %gather_fusion = bf16[576,2048]{1,0:T(8,128)(2,1)} fusion(bf16[192,2048]{1,0:T(8,128)(2,1)S(1)} %fusion.15, s32[1024]{0:T(1024)S(1)} %pad_clamp_fusion.1), kind=kCustom, calls=%fused_computation | custom fusion | bytes 4720896 | tf_op jit(solution)/shard_map/gather | solution.py:107
  23.0 1.3 dynamic-slice_select_fusion
  24.3 22.1 %all_to_all.10 = bf16[4,144,512]{2,1,0:T(8,128)(2,1)} all-to-all(bf16[4,144,512]{2,1,0:T(8,128)(2,1)S(1)} %dynamic-slice_select_fusion), channel_id=1, replica_groups=mesh['grp'=2,'ep'=4,'tp'=4] {'ep'}, dimensions={0} | all-to-all | bytes 1179648 | tf_op jit(solution)/shard_map/all_to_all | solution.py:113
  46.4 0.0 all-gather.5.cloned.1.call-update
  46.4 0.0 reduce-scatter.2.cloned.1.call-start
  46.5 23.3 %all-gather.5.cloned.1.call-done = bf16[4,144,2048]{2,1,0:T(8,128)(2,1)} async-done(((bf16[4,144,512]{2,1,0:T(8,128)(2,1)}), bf16[4,144,2048]{2,1,0:T(8,128)(2,1)}) %all-gather.5.cloned.1.call-update) | async-done | bytes 2359312 | tf_op jit(solution)/shard_map/all_gather | solution.py:112
  69.7 4.7 %fusion.9 = f32[576,512]{1,0:T(8,128)} fusion(bf16[576,2048]{1,0:T(8,128)(2,1)} %bitcast.131, bf16[1,2048,512]{2,1,0:T(8,128)(2,1)} %param.25), kind=kOutput, calls=%fused_computation.15 | convolution fusion | flops 1207959552 | bytes 5636096 | tf_op jit(solution)/shard_map/dot_general | solution.py:120
  74.5 0.0 copy-done
  74.5 6.7 %convolution_convert_fusion = bf16[576,2048]{1,0:T(8,128)(2,1)} fusion(bf16[1,512,2048]{2,1,0:T(8,128)(2,1)S(1)} %copy-done, bf16[576,2048]{1,0:T(8,128)(2,1)} %bitcast.132, bf16[1,2048,512]{2,1,0:T(8,128)(2,1)} %param.26, f32[576,512]{1,0:T(8,128)} %fusion.9), kind=kOutput, calls=%fused_computation.9 | convolution fusion | flops 2418868224 | bytes 10092544 | tf_op jit(solution)/shard_map/dot_general | solution.py:123
  81.2 0.0 reduce-scatter.2.cloned.1.call-update
  81.2 0.0 copy-start.5
  81.2 0.0 all-gather.3.cloned.1.call-start
  81.3 0.8 copy-done.2
  82.1 0.1 fusion.43
  82.3 0.1 fusion.44
  82.4 0.1 copy.20
  82.5 0.1 copy.21
  82.7 0.1 broadcast_multiply_fusion.1
  82.8 0.6 add_convert_fusion
  83.4 0.1 copy.23
  83.5 0.1 copy.24
  83.6 0.0 copy-done.1
  83.6 0.1 copy.22
  83.8 0.0 copy-done.5
  83.8 0.1 mul.300
  83.8 0.8 constant_dynamic-slice_fusion
  84.7 0.1 copy.34
  84.8 0.1 bitcast_reduce_fusion.1
  84.9 0.1 multiply_multiply_fusion
  85.1 0.2 fusion.38
  85.3 13.9 %all_gather.12 = bf16[1024,128]{1,0:T(8,128)(2,1)S(1)} all-gather(bf16[256,128]{1,0:T(8,128)(2,1)S(1)} %get-tuple-element.2), channel_id=1, replica_groups=mesh['grp'=2,'ep'=4,'tp'=4] {'ep'}, dimensions={0}, use_global_device_ids=true | all-gather | bytes 327680 | tf_op jit(solution)/shard_map/all_gather | solution.py:72
  99.2 14.7 %all_gather.13 = bf16[1024,128]{0,1:T(8,128)(2,1)S(1)} all-gather(bf16[256,128]{0,1:T(8,128)(2,1)S(1)} %copy.34), channel_id=1, replica_groups=mesh['grp'=2,'ep'=4,'tp'=4] {'ep'}, dimensions={0}, use_global_device_ids=true | all-gather | bytes 327680 | tf_op jit(solution)/shard_map/all_gather | solution.py:73
  113.9 0.7 bitcast_reduce_fusion
  114.6 0.7 fusion.1
  115.3 0.0 copy-start.3
  115.3 0.0 copy-start.6
  115.4 1.6 %fusion.31 = bf16[1,128,256,4]{2,1,3,0:T(8,128)(2,1)} fusion(f32[1024,256,4]{1,0,2:T(8,128)S(1)} %get-tuple-element.14, f32[256,4]{0,1:T(4,128)S(1)} %get-tuple-element.13, bf16[1024,128]{0,1:T(8,128)(2,1)S(1)} %all_gather.13, f32[256,4]{0,1:T(4,128)S(1)} %get-tuple-element.10, f32[256,4]{0,1:T(4,128)S(1)} %get-tuple-element.9), kind=kOutput, calls=%fused_computation.30 | convolution fusion | flops 271974400 | bytes 4730880 | tf_op jit(solution)/shard_map/qkgn,nkd->qkgd/dot_general | solution.py:84
  117.0 0.0 all-gather.3.cloned.1.call-update
  117.0 0.0 reduce-scatter.2.cloned.1.call-done
  117.0 4.8 %all-to-all-start.1 = ((bf16[4,144,512]{2,1,0:T(8,128)(2,1)}), bf16[4,144,512]{2,1,0:T(8,128)(2,1)S(1)}, u32[]{:S(2)}, u32[]{:S(2)}) async-start(bf16[4,144,512]{2,1,0:T(8,128)(2,1)} %reduce-scatter.2.cloned.1.call-done), calls=%async_computation.2 | async-start | bytes 1179648 | tf_op jit(solution)/shard_map/all_to_all | solution.py:130
  121.8 0.1 copy.28
  122.0 12.0 %all-gather.3.cloned.1.call-done = bf16[256,2048]{0,1:T(8,128)(2,1)} async-done(((bf16[256,512]{0,1:T(8,128)(2,1)}), bf16[256,2048]{0,1:T(8,128)(2,1)}) %all-gather.3.cloned.1.call-update) | async-done | bytes 1048592 | tf_op jit(solution)/shard_map/all_gather | solution.py:90
  134.0 3.3 %convolution_convert_fusion.1 = bf16[256,512]{1,0:T(8,128)(2,1)} fusion(bf16[256,2048]{0,1:T(8,128)(2,1)} %all-gather.3.cloned.1.call-done, bf16[2048,512]{1,0:T(8,128)(2,1)} %param.19), kind=kOutput, calls=%fused_computation.28 | convolution fusion | flops 537001984 | bytes 3407872 | tf_op jit(solution)/shard_map/dot_general | solution.py:89
  137.3 0.0 all-to-all-done.1
  137.3 2.1 %gather_fusion.1 = bf16[384,512]{1,0:T(8,128)(2,1)S(1)} fusion(bf16[576,512]{1,0:T(8,128)(2,1)S(1)} %bitcast.122, s32[1024]{0:T(1024)S(1)} %pad_clamp_fusion), kind=kCustom, calls=%fused_computation.1 | custom fusion | bytes 787968 | tf_op jit(solution)/shard_map/gather | solution.py:132
  139.4 0.5 reshape.352
  139.9 1.7 %multiply_reduce_fusion = bf16[192,512]{1,0:T(8,128)(2,1)} fusion(f32[192,2,512]{2,1,0:T(2,128)S(1)} %reshape.352, f32[192,2]{1,0:T(8,128)S(1)} %copy.28), kind=kLoop, calls=%fused_computation.31 | loop fusion | flops 294912 | bytes 984576 | tf_op jit(solution)/shard_map/reduce_sum | solution.py:134
  (28 shorter events, 0.3 us)
Async XLA Ops:
  7.2 67.3 %copy-start = (bf16[1,512,2048]{2,1,0:T(8,128)(2,1)S(1)}, bf16[1,512,2048]{2,1,0:T(8,128)(2,1)}, u32[]{:S(2)}) copy-start(bf16[1,512,2048]{2,1,0:T(8,128)(2,1)} %param.27) | copy-start | bytes 6291460
  7.2 62.6 %all-gather.5.cloned.1.call-start = ((), (), s32[]{:S(2)}) async-start(), calls=%async_computation.4 | async-start | bytes 2949120 | tf_op jit(solution)/shard_map/all_gather | solution.py:112
  46.4 70.6 %reduce-scatter.2.cloned.1.call-start = ((), (), s32[]{:S(2)}) async-start(), calls=%async_computation.5 | async-start | bytes 2949120 | tf_op jit(solution)/shard_map/reduce_scatter | solution.py:126
  81.2 0.9 copy-start.2
  81.2 1.1 copy-start.4
  81.2 2.4 %copy-start.1 = (bf16[256,512]{1,0:T(8,128)(2,1)S(1)}, bf16[256,512]{1,0:T(8,128)(2,1)}, u32[]{:S(2)}) copy-start(bf16[256,512]{1,0:T(8,128)(2,1)} %param.14) | copy-start | bytes 786436
  81.2 2.5 %copy-start.5 = (f32[128]{0:T(128)S(1)}, f32[128]{0:T(128)}, u32[]{:S(2)}) copy-start(f32[128]{0:T(128)} %param.17) | copy-start | bytes 1540
  81.2 52.8 %all-gather.3.cloned.1.call-start = ((), (), s32[]{:S(2)}) async-start(), calls=%async_computation.3 | async-start | bytes 1310720 | tf_op jit(solution)/shard_map/all_gather | solution.py:90
  115.3 6.4 %copy-start.3 = (f32[192,2]{0,1:T(2,128)S(1)}, f32[192,2]{0,1:T(2,128)}, u32[]{:S(2)}) copy-start(f32[192,2]{0,1:T(2,128)} %param.23) | copy-start | bytes 4612
  115.3 6.5 %copy-start.6 = (f32[192]{0:T(256)S(1)}, f32[192]{0:T(256)}, u32[]{:S(2)}) copy-start(f32[192]{0:T(256)} %param.22) | copy-start | bytes 2308
  117.0 20.3 %all-to-all-start.1 = ((bf16[4,144,512]{2,1,0:T(8,128)(2,1)}), bf16[4,144,512]{2,1,0:T(8,128)(2,1)S(1)}, u32[]{:S(2)}, u32[]{:S(2)}) async-start(bf16[4,144,512]{2,1,0:T(8,128)(2,1)} %reduce-scatter.2.cloned.1.call-done), calls=%async_computation.2 | async-start | bytes 1179648 | tf_op jit(solution)/shard_map/all_to_all | solution.py:130
Sparse Core Ops, SparseCore 0:
  46.5 23.1 all-gather.4
  81.3 32.7 reduce-scatter.1
  117.1 16.8 all-gather.2
where the time goes:
time: 149 us; the launch traced here: 148 us
  blocking collectives  50.8 us (34%)
  waiting for transfers between devices  35.3 us (24%)
  matrix products  17.1 us (11%)
  local copies, waits for them, and re-layouts  15.8 us (11%)
  between operations  14.1 us (9%)
  other arithmetic  10.1 us (7%)
  starting transfers between devices  4.88 us (3%)
    all_gather x1, waiting for transfers between devices, per_device(): lax.all_gather(lax.all_to_all(mine, 'ep', split_axis=0, concat_axis=0, ti...  23.3 us
    all_to_all x1, blocking collectives, per_device(): lax.all_to_all(mine, 'ep', split_axis=0, concat_axis=0, tiled=True)  22.1 us
    all_gather x1, blocking collectives, per_device(): v_piece = lax.all_gather(v_mine, 'ep', axis=0, tiled=True)  14.7 us
    all_gather x1, blocking collectives, per_device(): k_piece = lax.all_gather(k_rot, 'ep', axis=0, tiled=True)  13.9 us
    all_gather x1, waiting for transfers between devices, per_device(): lax.all_gather(mixed, 'tp', axis=1, tiled=True)  12 us
    dot_general x1, matrix products, per_device(): jnp.dot(hidden, w_down[0], preferred_element_type=jnp.float32)  6.71 us
    all_to_all x1, starting transfers between devices, per_device(): back = lax.all_to_all(summed, 'ep', split_axis=0, concat_axis=0, tiled=True)  4.76 us
    dot_general x1, matrix products, per_device(): gate = jnp.dot(flat, w_gate[0], preferred_element_type=jnp.float32)  4.74 us
  transfers between devices with their start and end apart: 4, of which 2 were waited for; matrix products, arithmetic and copies ran while one was open for 6% of the time, Pallas kernels for 0%

commit v1 on v0

--- a/solution.py
+++ b/solution.py
@@ -8,6 +8,11 @@
 HEAD_DIM = 128
 GRID_W = 64
 TOPK = 2
+
+
+def gathered_along(x, axis, dim):
+    shards = lax.all_gather(x, axis)
+    return jnp.concatenate(shards, axis=dim)
 
 
 def head_norm(x, gain):
@@ -87,7 +92,7 @@
     top, total, acc = (new_top, total, acc)
     mixed = (acc / total[..., None]).astype(jnp.bfloat16).reshape(rows, heads_dev * HEAD_DIM)
     attn_out = jnp.dot(
-        lax.all_gather(mixed, "tp", axis=1, tiled=True), w_out, preferred_element_type=jnp.float32
+        gathered_along(mixed, "tp", 1), w_out, preferred_element_type=jnp.float32
     ).astype(jnp.bfloat16)
     count = moe_rows.shape[0]
     width = moe_rows.shape[1]

time: 149 us -> 151 us (1.013)
  local copies, waits for them, and re-layouts: 15.8 us -> 18.9 us
    all_gather x0 -> x1, local copies, waits for them, and re-layouts: none -> 2.27 us  [gathered_along(): shards = lax.all_gather(x, axis)]
  transfers between devices with their start and end apart: 4 -> 4, of which waited for: 2 -> 2; matrix products, arithmetic and copies ran while one was open for 6% -> 8% of each run, Pallas kernels for 0% -> 0%
where the time goes in v1:
time: 151 us
  blocking collectives  50.8 us (34%)
  waiting for transfers between devices  35.3 us (23%)
  local copies, waits for them, and re-layouts  18.9 us (13%)
  matrix products  16.4 us (11%)
  between operations  14.1 us (9%)
  other arithmetic  10.1 us (7%)
  starting transfers between devices  4.88 us (3%)
    all_gather x1, waiting for transfers between devices, per_device(): lax.all_gather(lax.all_to_all(mine, 'ep', split_axis=0, concat_axis=0, ti...  23.3 us
    all_to_all x1, blocking collectives, per_device(): lax.all_to_all(mine, 'ep', split_axis=0, concat_axis=0, tiled=True)  22.1 us
    all_gather x1, blocking collectives, per_device(): v_piece = lax.all_gather(v_mine, 'ep', axis=0, tiled=True)  14.7 us
    all_gather x1, blocking collectives, per_device(): k_piece = lax.all_gather(k_rot, 'ep', axis=0, tiled=True)  13.9 us
    all_gather x1, waiting for transfers between devices, gathered_along(): shards = lax.all_gather(x, axis)  12 us
    dot_general x1, matrix products, per_device(): jnp.dot(hidden, w_down[0], preferred_element_type=jnp.float32)  6.71 us
    all_to_all x1, starting transfers between devices, per_device(): back = lax.all_to_all(summed, 'ep', split_axis=0, concat_axis=0, tiled=True)  4.76 us
    dot_general x1, matrix products, per_device(): gate = jnp.dot(flat, w_gate[0], preferred_element_type=jnp.float32)  4.74 us
  transfers between devices with their start and end apart: 4, of which 2 were waited for; matrix products, arithmetic and copies ran while one was open for 8% of the time, Pallas kernels for 0%

profile of v1, /device:TPU:0, one launch (start us, length us, event | category | flops | bytes accessed | tf_op | source)
XLA Modules:
  0.0 150.6 jit_solution(17899786953340325063)
XLA Ops:
  7.2 0.0 copy-start
  7.2 0.0 all-gather.5.cloned.1.call-start
  7.2 0.9 copy.57
  8.2 0.1 eq.32
  8.3 0.1 eq.28
  8.5 0.7 broadcast_multiply_fusion.2
  9.2 1.2 reduce-window.6
  10.4 0.2 slice_reduce_fusion
  10.6 0.2 reduce-window.9
  10.8 0.1 add_bitcast_fusion
  10.8 0.1 copy.56
  11.0 0.1 mul.316
  11.2 2.9 %scatter_custom_fusion.1 = s32[576]{0:T(1024)S(1)} fusion(s32[384]{0:T(512)S(1)} %fusion.58, s32[384]{0:T(512)S(1)} %add_select_fusion, s32[]{:T(128)} %constant.95.clone.1), kind=kCustom, calls=%fused_computation.81 | custom fusion | bytes 2308 | tf_op jit(solution)/shard_map/scatter | solution.py:110
  14.1 1.4 fusion.13
  15.5 2.0 %scatter_custom_fusion = pred[576]{0:T(1024)(128)(4,1)S(1)} fusion(s32[384]{0:T(512)S(1)} %fusion.58, pred[384]{0:T(512)(128)(4,1)S(1)} %broadcast.278, pred[]{:T(512)} %constant.115.clone.1), kind=kCustom, calls=%fused_computation.86 | custom fusion | bytes 577 | tf_op jit(solution)/shard_map/scatter | solution.py:111
  17.5 0.1 broadcast_in_dim.24
  17.6 1.4 fusion.15
  19.0 4.0 %gather_fusion = bf16[576,2048]{1,0:T(8,128)(2,1)} fusion(bf16[192,2048]{1,0:T(8,128)(2,1)S(1)} %fusion.15, s32[1024]{0:T(1024)S(1)} %pad_clamp_fusion.1), kind=kCustom, calls=%fused_computation | custom fusion | bytes 4720896 | tf_op jit(solution)/shard_map/gather | solution.py:112
  23.0 1.3 dynamic-slice_select_fusion
  24.3 22.1 %all_to_all.10 = bf16[4,144,512]{2,1,0:T(8,128)(2,1)} all-to-all(bf16[4,144,512]{2,1,0:T(8,128)(2,1)S(1)} %dynamic-slice_select_fusion), channel_id=1, replica_groups=mesh['grp'=2,'ep'=4,'tp'=4] {'ep'}, dimensions={0} | all-to-all | bytes 1179648 | tf_op jit(solution)/shard_map/all_to_all | solution.py:118
  46.4 0.0 all-gather.5.cloned.1.call-update
  46.4 0.0 reduce-scatter.2.cloned.1.call-start
  46.5 23.3 %all-gather.5.cloned.1.call-done = bf16[4,144,2048]{2,1,0:T(8,128)(2,1)} async-done(((bf16[4,144,512]{2,1,0:T(8,128)(2,1)}), bf16[4,144,2048]{2,1,0:T(8,128)(2,1)}) %all-gather.5.cloned.1.call-update) | async-done | bytes 2359312 | tf_op jit(solution)/shard_map/all_gather | solution.py:117
  69.7 4.7 %fusion.9 = f32[576,512]{1,0:T(8,128)} fusion(bf16[576,2048]{1,0:T(8,128)(2,1)} %bitcast.135, bf16[1,2048,512]{2,1,0:T(8,128)(2,1)} %param.25), kind=kOutput, calls=%fused_computation.15 | convolution fusion | flops 1207959552 | bytes 5636096 | tf_op jit(solution)/shard_map/dot_general | solution.py:125
  74.5 6.7 %convolution_convert_fusion = bf16[576,2048]{1,0:T(8,128)(2,1)} fusion(bf16[1,512,2048]{2,1,0:T(8,128)(2,1)S(1)} %copy-done, bf16[576,2048]{1,0:T(8,128)(2,1)} %bitcast.136, bf16[1,2048,512]{2,1,0:T(8,128)(2,1)} %param.26, f32[576,512]{1,0:T(8,128)} %fusion.9), kind=kOutput, calls=%fused_computation.9 | convolution fusion | flops 2418868224 | bytes 10092544 | tf_op jit(solution)/shard_map/dot_general | solution.py:128
  81.2 0.0 reduce-scatter.2.cloned.1.call-update
  81.2 0.0 copy-start.5
  81.2 0.0 all-gather.3.cloned.1.call-start
  81.3 0.8 copy-done.2
  82.1 0.1 fusion.43
  82.3 0.1 fusion.44
  82.4 0.1 copy.45
  82.5 0.1 copy.46
  82.7 0.1 broadcast_multiply_fusion.1
  82.8 0.6 add_convert_fusion
  83.4 0.1 copy.48
  83.5 0.1 copy.49
  83.6 0.0 copy-done.1
  83.6 0.1 copy.47
  83.8 0.1 mul.300
  83.8 0.8 constant_dynamic-slice_fusion
  84.7 0.1 copy.61
  84.8 0.1 bitcast_reduce_fusion.1
  84.9 0.1 multiply_multiply_fusion
  85.1 0.2 fusion.38
  85.3 13.9 %all_gather.12 = bf16[1024,128]{1,0:T(8,128)(2,1)S(1)} all-gather(bf16[256,128]{1,0:T(8,128)(2,1)S(1)} %get-tuple-element.2), channel_id=1, replica_groups=mesh['grp'=2,'ep'=4,'tp'=4] {'ep'}, dimensions={0}, use_global_device_ids=true | all-gather | bytes 327680 | tf_op jit(solution)/shard_map/all_gather | solution.py:77
  99.2 14.7 %all_gather.13 = bf16[1024,128]{0,1:T(8,128)(2,1)S(1)} all-gather(bf16[256,128]{0,1:T(8,128)(2,1)S(1)} %copy.61), channel_id=1, replica_groups=mesh['grp'=2,'ep'=4,'tp'=4] {'ep'}, dimensions={0}, use_global_device_ids=true | all-gather | bytes 327680 | tf_op jit(solution)/shard_map/all_gather | solution.py:78
  113.9 0.7 bitcast_reduce_fusion
  114.6 0.7 fusion.1
  115.3 0.0 copy-start.3
  115.3 0.0 copy-start.6
  115.4 0.9 fusion.31
  116.3 0.8 copy.53
  117.1 0.0 all-gather.3.cloned.1.call-update
  117.1 0.0 reduce-scatter.2.cloned.1.call-done
  117.2 4.8 %all-to-all-start.1 = ((bf16[4,144,512]{2,1,0:T(8,128)(2,1)}), bf16[4,144,512]{2,1,0:T(8,128)(2,1)S(1)}, u32[]{:S(2)}, u32[]{:S(2)}) async-start(bf16[4,144,512]{2,1,0:T(8,128)(2,1)} %reduce-scatter.2.cloned.1.call-done), calls=%async_computation.2 | async-start | bytes 1179648 | tf_op jit(solution)/shard_map/all_to_all | solution.py:135
  122.0 0.1 copy.55
  122.1 12.0 %all-gather.3.cloned.1.call-done = bf16[4,256,512]{2,1,0:T(8,128)(2,1)} async-done(((bf16[1,256,512]{2,1,0:T(8,128)(2,1)}), bf16[4,256,512]{2,1,0:T(8,128)(2,1)}) %all-gather.3.cloned.1.call-update) | async-done | bytes 1048592 | tf_op jit(solution)/shard_map/all_gather | solution.py:14
  134.1 2.3 %copy.54 = bf16[4,256,512]{1,2,0:T(8,128)(2,1)} copy(bf16[4,256,512]{2,1,0:T(8,128)(2,1)} %all-gather.3.cloned.1.call-done) | data formatting | bytes 2097152 | tf_op jit(solution)/shard_map/all_gather | solution.py:14
  136.4 3.3 %convolution_convert_fusion.1 = bf16[256,512]{1,0:T(8,128)(2,1)} fusion(bf16[256,2048]{0,1:T(8,128)(2,1)} %bitcast.129, bf16[2048,512]{1,0:T(8,128)(2,1)} %param.19), kind=kOutput, calls=%fused_computation.28 | convolution fusion | flops 537001984 | bytes 3407872 | tf_op jit(solution)/shard_map/dot_general | solution.py:94
  139.8 0.0 all-to-all-done.1
  139.8 2.1 %gather_fusion.1 = bf16[384,512]{1,0:T(8,128)(2,1)S(1)} fusion(bf16[576,512]{1,0:T(8,128)(2,1)S(1)} %bitcast.125, s32[1024]{0:T(1024)S(1)} %pad_clamp_fusion), kind=kCustom, calls=%fused_computation.1 | custom fusion | bytes 787968 | tf_op jit(solution)/shard_map/gather | solution.py:137
  141.8 0.5 reshape.356
  142.3 1.7 %multiply_reduce_fusion = bf16[192,512]{1,0:T(8,128)(2,1)} fusion(f32[192,2,512]{2,1,0:T(2,128)S(1)} %reshape.356, f32[192,2]{1,0:T(8,128)S(1)} %copy.55), kind=kLoop, calls=%fused_computation.31 | loop fusion | flops 294912 | bytes 984576 | tf_op jit(solution)/shard_map/reduce_sum | solution.py:139
  (30 shorter events, 0.3 us)
Async XLA Ops:
  7.2 67.3 %copy-start = (bf16[1,512,2048]{2,1,0:T(8,128)(2,1)S(1)}, bf16[1,512,2048]{2,1,0:T(8,128)(2,1)}, u32[]{:S(2)}) copy-start(bf16[1,512,2048]{2,1,0:T(8,128)(2,1)} %param.27) | copy-start | bytes 6291460
  7.2 62.6 %all-gather.5.cloned.1.call-start = ((), (), s32[]{:S(2)}) async-start(), calls=%async_computation.4 | async-start | bytes 2949120 | tf_op jit(solution)/shard_map/all_gather | solution.py:117
  46.4 70.7 %reduce-scatter.2.cloned.1.call-start = ((), (), s32[]{:S(2)}) async-start(), calls=%async_computation.5 | async-start | bytes 2949120 | tf_op jit(solution)/shard_map/reduce_scatter | solution.py:131
  81.2 0.9 copy-start.2
  81.2 1.1 copy-start.4
  81.2 2.4 %copy-start.1 = (bf16[256,512]{1,0:T(8,128)(2,1)S(1)}, bf16[256,512]{1,0:T(8,128)(2,1)}, u32[]{:S(2)}) copy-start(bf16[256,512]{1,0:T(8,128)(2,1)} %param.14) | copy-start | bytes 786436
  81.2 2.5 %copy-start.5 = (f32[128]{0:T(128)S(1)}, f32[128]{0:T(128)}, u32[]{:S(2)}) copy-start(f32[128]{0:T(128)} %param.17) | copy-start | bytes 1540
  81.2 52.9 %all-gather.3.cloned.1.call-start = ((), (), s32[]{:S(2)}) async-start(), calls=%async_computation.3 | async-start | bytes 1310720 | tf_op jit(solution)/shard_map/all_gather | solution.py:14
  115.3 6.6 %copy-start.3 = (f32[192,2]{0,1:T(2,128)S(1)}, f32[192,2]{0,1:T(2,128)}, u32[]{:S(2)}) copy-start(f32[192,2]{0,1:T(2,128)} %param.23) | copy-start | bytes 4612
  115.3 6.6 %copy-start.6 = (f32[192]{0:T(256)S(1)}, f32[192]{0:T(256)}, u32[]{:S(2)}) copy-start(f32[192]{0:T(256)} %param.22) | copy-start | bytes 2308
  117.2 22.6 %all-to-all-start.1 = ((bf16[4,144,512]{2,1,0:T(8,128)(2,1)}), bf16[4,144,512]{2,1,0:T(8,128)(2,1)S(1)}, u32[]{:S(2)}, u32[]{:S(2)}) async-start(bf16[4,144,512]{2,1,0:T(8,128)(2,1)} %reduce-scatter.2.cloned.1.call-done), calls=%async_computation.2 | async-start | bytes 1179648 | tf_op jit(solution)/shard_map/all_to_all | solution.py:135
Sparse Core Ops, SparseCore 0:
  46.5 23.1 all-gather.4
  81.3 32.7 reduce-scatter.1
  117.2 16.8 all-gather.2
